TPU v7x, 32 devices: a whole 2x2x4 slice. The times are simulated.
32 devices in a mesh: sp: 16 (over z, y, x), tp: 2 (over core).
Axes of the slice: x: 2, y: 2, z: 4, core: 2. Of those that a mesh axis runs over, the one named last changes fastest.
Arguments:
- queries: bfloat16 [4096, 2048], P('sp', 'tp'), may hold values from -6 to 6
- keys: bfloat16 [4096, 2048], P('sp', 'tp'), may hold values from -6 to 6
- hidden: bfloat16 [4096, 2048], P('sp'), may hold values from -6 to 6
- value_weight: bfloat16 [2048, 2048], P(None, 'tp'), may hold values from -0.125 to 0.125
- beta_pre: float32 [4096, 16], P('sp', 'tp'), may hold values from -9 to 3
- decay_pre: float32 [4096, 16], P('sp', 'tp'), may hold values from -5 to 4
- decay_rate: float32 [16], P('tp'), may hold values from 0 to 0.06
- out_grad: bfloat16 [4096, 2048], P('sp', 'tp'), may hold values from -6 to 6
Outputs:
- d_queries: bfloat16 [4096, 2048], P('sp', 'tp')
- d_keys: bfloat16 [4096, 2048], P('sp', 'tp')
- d_beta: float32 [4096, 16], P('sp', 'tp')
- d_decay: float32 [4096, 16], P('sp', 'tp')
- d_hidden: bfloat16 [4096, 2048], P(('sp', 'tp'))
- d_weight: float32 [2048, 2048], P('sp', 'tp')
All inputs are finite; a program needn't handle non-finite values.
Results may differ from a plain program's by a relative error of at most 0.022.
Values may be sent and summed in bfloat16 or wider, within the bound.
A program may use at most 256 MiB of HBM per device.

v0:
```python
import functools

import jax
import jax.numpy as jnp
from jax import lax
from jax.experimental import pallas as pl
from jax.experimental.pallas import tpu as pltpu
from jax.sharding import PartitionSpec as P


f32 = jnp.float32
bf16 = jnp.bfloat16
norm_floor = 16.0


def mm(a, b, ca, cb):
    return lax.dot_general(
        a.astype(bf16), b.astype(bf16), (((ca,), (cb,)), ((), ())), preferred_element_type=f32
    )


def nn(a, b):
    return mm(a, b, 1, 0)


def nt(a, b):
    return mm(a, b, 1, 1)


def tn(a, b):
    return mm(a, b, 0, 0)


def nn3(a, b):
    a_hi, b_hi = a.astype(bf16), b.astype(bf16)
    a_lo, b_lo = a - a_hi.astype(f32), b - b_hi.astype(f32)
    return nn(a_hi, b_hi) + (nn(a_hi, b_lo) + nn(a_lo, b_hi))


def invert_unit_lower(lows):
    size = lows[0].shape[0]
    base = min(size, 128)
    ii = lax.broadcasted_iota(jnp.int32, (base, base), 0)
    jj = lax.broadcasted_iota(jnp.int32, (base, base), 1)
    masks = []
    width = 1
    while width < base:
        masks.append((ii // (2 * width) == jj // (2 * width)) & (ii // width != jj // width))
        width *= 2
    blocks = [
        low[start : start + base, start : start + base]
        for low in lows
        for start in range(0, size, base)
    ]
    inverses = [jnp.where(ii == jj, 1.0, 0.0) - jnp.where(masks[0], a, 0.0) for a in blocks]
    for mask in masks[1:]:
        inner = [nn3(jnp.where(mask, a, 0.0), inv) for a, inv in zip(blocks, inverses)]
        outer = [nn3(inv, mid) for inv, mid in zip(inverses, inner)]
        inverses = [inv - out for inv, out in zip(inverses, outer)]
    per = size // base
    while per > 1:
        width = size // per
        joined, inner = [], []
        for pair in range(0, len(inverses), 2):
            low = lows[pair // per]
            row = (pair % per + 1) * width
            inner.append(nn3(low[row : row + width, row - width : row], inverses[pair]))
        for pair in range(0, len(inverses), 2):
            first, second = inverses[pair], inverses[pair + 1]
            corner = -nn3(second, inner[pair // 2])
            top = jnp.concatenate([first, jnp.zeros_like(first)], axis=1)
            joined.append(
                jnp.concatenate([top, jnp.concatenate([corner, second], axis=1)], axis=0)
            )
        inverses = joined
        per //= 2
    return inverses


def unit(raw):
    return lax.rsqrt(jnp.sum(raw * raw, axis=-1, keepdims=True) + norm_floor)


def order(size):
    ii = lax.broadcasted_iota(jnp.int32, (size, size), 0)
    jj = lax.broadcasted_iota(jnp.int32, (size, size), 1)
    return ii >= jj, ii > jj


def first_phase_group(inputs):
    prepared = [first_before(*one) for one in inputs]
    inverses = invert_unit_lower([one[0] for one in prepared])
    return [
        first_after(inverse, one[1], *given)
        for inverse, one, given in zip(inverses, prepared, inputs)
    ]


def first_before(qr, kr, v, do, b, gc, gr, ge):
    k = kr * unit(kr)
    inclusive, strict = order(qr.shape[0])
    mask = jnp.where(inclusive, jnp.exp(jnp.minimum(gc - gr, 0.0)), 0.0)
    return jnp.where(strict, b * nt(k, k) * mask, 0.0), mask


def first_after(inverse, mask, qr, kr, v, do, b, gc, gr, ge):
    width = qr.shape[1]
    q = qr * (unit(qr) * width ** (-0.5))
    k = kr * unit(kr)
    eg = jnp.exp(gc)
    kd = k * jnp.exp(ge - gc)
    uw = nn(inverse, jnp.concatenate([b * v, (b * eg) * k], axis=1))
    qk = nt(q, k) * mask
    moved = tn(kd, uw)
    ii = lax.broadcasted_iota(jnp.int32, (width, width), 0)
    jj = lax.broadcasted_iota(jnp.int32, (width, width), 1)
    dv = v.shape[1]
    offset = moved[:, :dv]
    transition = jnp.where(ii == jj, jnp.exp(ge), 0.0) - moved[:, dv:]
    dw0 = tn(qk, do)
    own = tn(q * eg, do) - tn(uw[:, dv:], dw0)
    return inverse, uw, dw0, transition, offset, own


def value_phase(kr, inverse, dw0, end, gc, ge):
    kd = kr * (unit(kr) * jnp.exp(ge - gc))
    return tn(inverse, dw0 + nn(kd, end))


def last_phase(qr, kr, v, do, uw, dr, start, end, b, gc, gr, ge):
    width = qr.shape[1]
    dv = v.shape[1]
    rq, rk = unit(qr), unit(kr)
    scale = width ** (-0.5)
    q = qr * (rq * scale)
    k = kr * rk
    inclusive, strict = order(qr.shape[0])
    mask = jnp.where(inclusive, jnp.exp(jnp.minimum(gc - gr, 0.0)), 0.0)
    gram = jnp.where(strict, nt(k, k) * mask, 0.0)
    qk = nt(q, k) * mask
    eg = jnp.exp(gc)
    ekd = jnp.exp(ge - gc)
    rest = v - eg * nn(k, start)
    written = uw[:, :dv] - nn(uw[:, dv:], start)
    dp = nt(do, written)
    dqd = nt(do, start) * eg
    dkd = nt(written, end) * ekd
    dl = -nt(dr, written)
    dkg = nt(dr, start) * (-b * eg)
    dlg = dl * gram
    db = jnp.sum(dr * rest, axis=1, keepdims=True) + jnp.sum(dlg, axis=1, keepdims=True)
    dg = jnp.where(strict, dl * b * mask, 0.0)
    dqk = dp * mask
    logs = dlg * b + dp * qk
    dq = nn(dqk, k) + dqd
    dk = tn(dqk, q) + nn(dg, k) + tn(dg, k) + dkg + dkd
    kept = jnp.sum(dkd * k, axis=1, keepdims=True)
    gcol = jnp.sum(logs, axis=1, keepdims=True) + jnp.sum(dqd * q + dkg * k, axis=1, keepdims=True) - kept
    last = jnp.sum(kept, axis=0, keepdims=True) + jnp.exp(ge) * jnp.sum(
        jnp.sum(start * end, axis=1, keepdims=True), axis=0, keepdims=True
    )
    rows = lax.broadcasted_iota(jnp.int32, gcol.shape, 0)
    gcol = gcol + jnp.where(rows == gcol.shape[0] - 1, last, 0.0)
    grow = jnp.sum(logs, axis=0, keepdims=True)
    dqr = (rq * scale) * (dq - qr * (rq * rq * jnp.sum(qr * dq, axis=1, keepdims=True)))
    dkr = rk * (dk - kr * (rk * rk * jnp.sum(kr * dk, axis=1, keepdims=True)))
    return dqr, dkr, db, gcol, grow


def pick(ref, head):
    table = ref[...]
    lane = lax.broadcasted_iota(jnp.int32, table.shape, 1)
    return jnp.sum(jnp.where(lane == head, table, 0.0), axis=1, keepdims=True)


def put(ref, head, column):
    lane = lax.broadcasted_iota(jnp.int32, ref.shape, 1)
    ref[...] = jnp.where(lane == head, column, ref[...])


def gains(g_ref, row_ref, head):
    gr = row_ref[...]
    return pick(g_ref, head), gr, gr[:, gr.shape[1] - 1 :]


def lanes(ref, i, group):
    width = ref.shape[1] // group
    return ref.at[:, i * width : (i + 1) * width]


PEERS = 4
MESH = pl.DeviceIdType.MESH


class Place:
    def __init__(self, count):
        me = lax.axis_index("sp")
        self.chain = count // PEERS
        self.p, self.q = me % PEERS, me // PEERS
        self.x, self.y = self.p % 2, self.p // 2
        self.core = lax.axis_index("tp")

    def peer(self, j):
        return (self.y + j // 2) % 2 * 2 + (self.x + j % 2) % 2

    def at_peer(self, j):
        return (self.q * PEERS + self.peer(j), self.core)

    def at_group(self, q):
        return (q * PEERS + self.p, self.core)

    def greet(self, others):
        barrier = pltpu.get_barrier_semaphore()
        for other in others:
            pl.semaphore_signal(barrier, inc=1, device_id=other, device_id_type=MESH)
        pl.semaphore_wait(barrier, len(others))

    def ring(self):
        return [self.at_group((self.q + 1) % self.chain), self.at_group((self.q + self.chain - 1) % self.chain)]


def remote(src, dst, send, recv, device):
    return pltpu.make_async_remote_copy(
        src_ref=src, dst_ref=dst, send_sem=send, recv_sem=recv, device_id=device, device_id_type=MESH
    )


def split(a, b, ca):
    hi = b.astype(bf16)
    return mm(a, hi, ca, 0) + mm(a, b - hi.astype(f32), ca, 0)


def head_lanes(ref, head, width):
    return ref.at[:, pl.ds(pl.multiple_of(head * width, width), width)]


def front_kernel(
    count, q, k, v, do, b, g, row, hid,
    inv_o, uw_o, dw_o, start_o, end_o, hid_o,
    pack, gat, trans, state_out, state_in, back,
    map_send, map_recv, hid_send, hid_recv, chain_send, chain_recv, back_send, back_recv,
):
    at = Place(count)
    heads = row.shape[0]
    own = heads // PEERS
    dk = q.shape[1] // heads
    dv = v.shape[1] // heads
    at.greet([at.at_peer(j) for j in range(1, PEERS)] + at.ring())
    for j in (1, 2, 3):
        remote(hid.at[at.peer(j)], hid_o.at[j], hid_send.at[j], hid_recv.at[j], at.at_peer(j)).start()

    def maps_copy(j):
        return remote(pack.at[j], gat.at[j], map_send.at[j], map_recv.at[j], at.at_peer(j))

    def local(t, carry):
        given, places = [], []
        for half in range(2):
            j = 3 - half - 2 * t
            for i in range(own):
                head = at.peer(j) * own + i
                places.append((j, i, head))
                gc, gr, ge = gains(g, row.at[head], head)
                given.append(
                    [head_lanes(a, head, dk)[...].astype(f32) for a in (q, k)]
                    + [head_lanes(a, head, dv)[...].astype(f32) for a in (v, do)]
                    + [pick(b, head), gc, gr, ge]
                )
        for (j, i, head), result in zip(places, first_phase_group(given)):
            inverse, uw, dw0, transition, offset, mine = result
            inv_o[head] = inverse.astype(inv_o.dtype)
            uw_o[head] = uw
            dw_o[head] = dw0
            pack[j, i, :, :dk] = transition.astype(bf16)
            pack[j, i, :, dk : dk + dv] = offset.astype(bf16)
            pack[j, i, :, dk + dv :] = mine.astype(bf16)
        maps_copy(3 - 2 * t).start()

        @pl.when(t == 0)
        def _():
            maps_copy(2).start()

        return carry

    lax.fori_loop(0, 2, local, 0)
    gat[0] = pack[0]
    hid_o[0] = hid[at.p]
    for j in (3, 2, 1):
        maps_copy(j).wait_recv()

    def span(s, i):
        j = (at.y + s // 2) % 2 * 2 + (at.x + s % 2) % 2
        return gat.at[j, i]

    def part(ref, n):
        return ref[:, (0, dk, dk + dv)[n] : (dk, dk + dv, dk + 2 * dv)[n]]

    for i in range(own):
        total, offset, grad = part(span(0, i), 0).astype(f32), part(span(0, i), 1).astype(f32), 0
        for s in range(1, PEERS):
            offset = split(part(span(s, i), 0), offset, 1) + part(span(s, i), 1).astype(f32)
            total = split(part(span(s, i), 0), total, 1)
        grad = part(span(PEERS - 1, i), 2).astype(f32)
        for s in range(PEERS - 2, -1, -1):
            grad = split(part(span(s, i), 0), grad, 0) + part(span(s, i), 2).astype(f32)
        hi = total.astype(bf16)
        trans[i, 0] = hi
        trans[i, 1] = (total - hi.astype(f32)).astype(bf16)
        trans[i, 2] = offset.astype(bf16)
        trans[i, 3] = grad.astype(bf16)

    last = at.chain - 1

    def chain_copy(kind, i):
        to = (at.q + 1) % at.chain if kind == 0 else (at.q + at.chain - 1) % at.chain
        return remote(
            state_out.at[kind, i], state_in.at[kind, i],
            chain_send.at[kind, i], chain_recv.at[kind, i], at.at_group(to),
        )

    def back_copy(kind, j):
        landing = (start_o, end_o)[kind].at[pl.ds(at.p * own, own)]
        return remote(back.at[kind, j], landing, back_send.at[kind, j], back_recv.at[kind, j], at.at_peer(j))

    def run(kind):
        first, end = (0, last) if kind == 0 else (last, 0)
        states = []
        for i in range(own):
            @pl.when(at.q == first)
            def _():
                state_in[kind, i] = jnp.zeros((dk, dv), bf16)

            @pl.when(at.q != first)
            def _():
                chain_copy(kind, i).wait_recv()

            state = state_in[kind, i]

            @pl.when(at.q != end)
            def _():
                ca = 1 - kind
                moved = mm(trans[i, 0], state, ca, 0) + mm(trans[i, 1], state, ca, 0)
                state_out[kind, i] = (moved + trans[i, 2 + kind].astype(f32)).astype(bf16)
                chain_copy(kind, i).start()

            states.append(state.astype(f32))
        order = list(range(PEERS)) if kind == 0 else list(range(PEERS - 1, -1, -1))
        for s in order:
            j = (at.y + s // 2) % 2 * 2 + (at.x + s % 2) % 2
            for i in range(own):
                back[kind, j, i] = states[i].astype(bf16)

            @pl.when(j != 0)
            def _():
                back_copy(kind, j).start()

            if s != order[-1]:
                states = [
                    split(part(span(s, i), 0), states[i], 1 - kind) + part(span(s, i), 1 + kind).astype(f32)
                    for i in range(own)
                ]

    half = at.chain // 2

    @pl.when(at.q < half)
    def _():
        run(0)

    run(1)

    @pl.when(at.q >= half)
    def _():
        run(0)

    start_o[pl.ds(at.p * own, own)] = back[0, 0]
    end_o[pl.ds(at.p * own, own)] = back[1, 0]

    def arrival(kind, j):
        landing = (start_o, end_o)[kind].at[pl.ds(at.peer(j) * own, own)]
        return remote(back.at[kind, j], landing, back_send.at[kind, j], back_recv.at[kind, j], at.at_peer(j))

    for j in (1, 2, 3):
        for kind in range(2):
            arrival(kind, j).wait()
        remote(hid.at[at.peer(j)], hid_o.at[j], hid_send.at[j], hid_recv.at[j], at.at_peer(j)).wait()
        maps_copy(j).wait_send()
    for i in range(own):
        @pl.when(at.q != last)
        def _():
            chain_copy(0, i).wait_send()

        @pl.when(at.q != 0)
        def _():
            chain_copy(1, i).wait_send()


def value_kernel(group, k, inv, dw, end, b, g, row, dr_o, dv_o):
    for i in range(group):
        head = pl.program_id(0) * group + i
        gc, _, ge = gains(g, row.at[i], head)
        bc = pick(b, head)
        dr = value_phase(lanes(k, i, group)[...].astype(f32), inv[i], dw[i], end[i], gc, ge)
        dr_o[i] = dr
        lanes(dv_o, i, group)[...] = (bc * dr).astype(bf16)


def last_kernel(group, q, k, v, do, uw, dr, start, end, b, g, row, dq_o, dk_o, db_o, gc_o, gr_o):
    @pl.when(pl.program_id(0) == 0)
    def _():
        db_o[...] = jnp.zeros_like(db_o)
        gc_o[...] = jnp.zeros_like(gc_o)

    for i in range(group):
        head = pl.program_id(0) * group + i
        gc, gr, ge = gains(g, row.at[i], head)
        raw = [lanes(a, i, group)[...].astype(f32) for a in (q, k, v, do)]
        dqr, dkr, db, gcol, grow = last_phase(
            *raw, uw[i], dr[i], start[i].astype(f32), end[i].astype(f32), pick(b, head), gc, gr, ge
        )
        lanes(dq_o, i, group)[...] = dqr.astype(bf16)
        lanes(dk_o, i, group)[...] = dkr.astype(bf16)
        put(db_o, head, db)
        put(gc_o, head, gcol)
        gr_o[i] = grow


def exchange(value, axis, bit):
    count = lax.axis_size(axis)
    return lax.ppermute(value, axis, [(i, i ^ bit) for i in range(count)])


def bit_of(axis, bit):
    return (lax.axis_index(axis) >> bit) & 1


class Halving:
    def __init__(self, hidden, grads, bits, sequence):
        self.grads, self.sequence = grads, sequence
        self.length, self.rows, self.count = hidden.shape[0], hidden.shape[1], 1 << bits
        self.left = sorted(range(bits), reverse=True)
        self.axis = 1 + self.left.index(sequence[0])
        self.mine = bit_of("sp", sequence[0])
        self.split = hidden.reshape((self.length,) + (2,) * bits + (self.rows // self.count,))
        self.send = self.product(1 - self.mine).astype(bf16)

    def product(self, side):
        piece = lax.dynamic_index_in_dim(self.split, side, self.axis, False)
        piece = piece.reshape(self.length, self.rows // 2)
        return lax.dot_general(
            piece, self.grads, (((0,), (0,)), ((), ())), preferred_element_type=f32
        )

    def finish(self, send):
        left = list(self.left)
        got = exchange(send, "sp", 1 << self.sequence[0])
        total = self.product(self.mine) + got.astype(f32)
        left.remove(self.sequence[0])
        for bit in self.sequence[1:]:
            place = left.index(bit)
            mine = bit_of("sp", bit)
            shaped = total.reshape(1 << place, 2, -1, total.shape[-1])
            send = lax.dynamic_index_in_dim(shaped, 1 - mine, 1, False)
            keep = lax.dynamic_index_in_dim(shaped, mine, 1, False)
            got = exchange(send.astype(bf16), "sp", 1 << bit)
            total = keep + got.astype(f32)
            left.remove(bit)
        return total.reshape(self.rows // self.count, -1)


def plan_weight(hidden, grads, count):
    bits = count.bit_length() - 1
    low = bits // 2
    order_a = list(range(bits))
    order_b = order_a[:low][::-1] + order_a[low:]
    order_c = order_a[low:] + order_a[:low]
    width = grads.shape[1]
    cut = max(width * 3 // 8 // 128 * 128, 1)
    groups = [(0, cut, order_a), (cut, 2 * cut, order_b), (2 * cut, width, order_c)]
    return [Halving(hidden, grads[:, lo:hi], bits, seq) for lo, hi, seq in groups]


def reduce_hidden(grads, weight):
    cores = lax.axis_size("tp")
    assert cores == 2
    half = grads.shape[0] // cores
    me = lax.axis_index("tp")

    def product(side):
        rows = lax.dynamic_slice_in_dim(grads, side * half, half, 0)
        return lax.dot_general(
            rows, weight, (((1,), (1,)), ((), ())), preferred_element_type=f32
        ).astype(bf16)

    send = product(1 - me)
    got = exchange(send, "tp", 1)
    return (product(me).astype(f32) + got.astype(f32)).astype(bf16)


def compute(queries, keys, hidden, value_weight, beta_pre, decay_pre, decay_rate, out_grad):
    heads = decay_rate.shape[0]
    length, dk = queries.shape[0], queries.shape[1] // heads
    dv = value_weight.shape[1] // heads
    count = lax.axis_size("sp")
    group = 4 if heads % 4 == 0 else 1

    values = jnp.dot(hidden, value_weight, preferred_element_type=f32).astype(bf16)
    beta = jax.nn.sigmoid(beta_pre)
    log_decay = -decay_rate[None, :] * jax.nn.softplus(decay_pre)
    inclusive = jnp.tril(jnp.ones((length, length), f32))
    sums = jnp.dot(inclusive, log_decay, precision=lax.Precision.HIGHEST)
    sums_row = sums.T.reshape(heads, 1, length)

    wide = lambda n: pl.BlockSpec((length, group * n), lambda h: (0, h))
    per_head = lambda r, c: pl.BlockSpec((group, r, c), lambda h: (h, 0, 0))
    table = pl.BlockSpec((length, heads), lambda h: (0, 0))
    shape = jax.ShapeDtypeStruct
    params = pltpu.CompilerParams(dimension_semantics=("arbitrary",))

    own = heads // PEERS
    chain = count // PEERS
    rows = hidden.shape[1] // count
    pieces = hidden.reshape(length, chain, PEERS, rows)
    pieces = jnp.moveaxis(pieces, 2, 0).reshape(PEERS, length, chain * rows)
    vmem = pl.BlockSpec(memory_space=pltpu.VMEM)
    dma = pltpu.SemaphoreType.DMA
    inverse, uw, dw0, start, end, _ = pl.pallas_call(
        functools.partial(front_kernel, count),
        in_specs=[vmem] * 8,
        out_specs=[vmem] * 6,
        out_shape=[
            shape((heads, length, length), bf16), shape((heads, length, dv + dk), f32),
            shape((heads, length, dv), f32), shape((heads, dk, dv), bf16),
            shape((heads, dk, dv), bf16), shape(pieces.shape, bf16),
        ],
        scratch_shapes=[
            pltpu.VMEM((PEERS, own, dk, dk + 2 * dv), bf16),
            pltpu.VMEM((PEERS, own, dk, dk + 2 * dv), bf16),
            pltpu.VMEM((own, 4, dk, dk), bf16),
            pltpu.VMEM((2, own, dk, dv), bf16),
            pltpu.VMEM((2, own, dk, dv), bf16),
            pltpu.VMEM((2, PEERS, own, dk, dv), bf16),
            dma((PEERS,)), dma((PEERS,)), dma((PEERS,)), dma((PEERS,)),
            dma((2, own)), dma((2, own)), dma((2, PEERS)), dma((2, PEERS)),
        ],
        compiler_params=pltpu.CompilerParams(collective_id=0, has_side_effects=True),
        cost_estimate=pl.CostEstimate(flops=1 << 30, bytes_accessed=1 << 23, transcendentals=0),
        name="front",
    )(queries, keys, values, out_grad, beta, sums, sums_row, pieces)

    dr, grad_values = pl.pallas_call(
        functools.partial(value_kernel, group),
        grid=(heads // group,),
        in_specs=[
            wide(dk), per_head(length, length), per_head(length, dv), per_head(dk, dv),
            table, table, per_head(1, length),
        ],
        out_specs=[per_head(length, dv), wide(dv)],
        out_shape=[shape((heads, length, dv), f32), shape((length, heads * dv), bf16)],
        compiler_params=params,
        name="value",
    )(keys, inverse, dw0, end, beta, sums, sums_row)

    plans = plan_weight(hidden, grad_values, count)
    sends, dr, start = lax.optimization_barrier(([plan.send for plan in plans], dr, start))
    d_weight = jnp.concatenate([plan.finish(x) for plan, x in zip(plans, sends)], axis=1)
    d_hidden = reduce_hidden(grad_values, value_weight)

    d_queries, d_keys, db, gcol, grow = pl.pallas_call(
        functools.partial(last_kernel, group),
        grid=(heads // group,),
        in_specs=[
            wide(dk), wide(dk), wide(dv), wide(dv), per_head(length, dv + dk),
            per_head(length, dv), per_head(dk, dv), per_head(dk, dv),
            table, table, per_head(1, length),
        ],
        out_specs=[wide(dk), wide(dk), table, table, per_head(1, length)],
        out_shape=[
            shape(queries.shape, bf16), shape(keys.shape, bf16), shape((length, heads), f32),
            shape((length, heads), f32), shape((heads, 1, length), f32),
        ],
        compiler_params=params,
        cost_estimate=pl.CostEstimate(
            flops=heads * 13 * 2 * length * length * dk, bytes_accessed=12 << 20, transcendentals=0
        ),
        name="last",
    )(queries, keys, values, out_grad, uw, dr, start, end, beta, sums, sums_row)
    grad_sums = gcol - grow.reshape(heads, length).T
    grad_log = jnp.dot(inclusive.T, grad_sums, precision=lax.Precision.HIGHEST)
    d_decay = grad_log * (-decay_rate[None, :] * jax.nn.sigmoid(decay_pre))
    d_beta = db * beta * (1.0 - beta)
    return (d_queries, d_keys, d_beta, d_decay, d_hidden, d_weight)


def solution(mesh):
    return jax.shard_map(
        compute,
        mesh=mesh,
        in_specs=(
            P("sp", "tp"), P("sp", "tp"), P("sp", None), P(None, "tp"),
            P("sp", "tp"), P("sp", "tp"), P("tp"), P("sp", "tp"),
        ),
        out_specs=(
            P("sp", "tp"), P("sp", "tp"), P("sp", "tp"), P("sp", "tp"),
            P(("sp", "tp"), None), P("sp", "tp"),
        ),
        check_vma=False,
    )
```

profile of v0, /device:TPU:0, one launch (start us, length us, event | category | flops | bytes accessed | tf_op | source)
XLA Modules:
  0.0 138.0 jit_solution(2045073813025004637)
XLA Ops:
  0.6 1.9 %reshape.122 = bf16[256,4,4,128]{3,2,1,0:T(4,128)(2,1)S(1)} reshape(bf16[256,2048]{1,0:T(8,128)(2,1)} %param.10) | data formatting | bytes 2097152 | tf_op jit(solution)/shard_map/reshape | solution.py:521
  2.5 0.0 copy-start.2
  2.5 0.0 copy-start.4
  2.6 0.0 copy-start.3
  2.6 4.2 %convolution_convert_fusion.5.v = bf16[256,1024]{1,0:T(8,128)(2,1)} fusion(bf16[256,2048]{1,0:T(8,128)(2,1)S(1)} %copy-done.1, bf16[2048,1024]{1,0:T(8,128)(2,1)} %param.11), kind=kOutput, calls=%fused_computation.8 | convolution fusion | flops 1074003968 | bytes 5767168 | tf_op jit(solution)/shard_map/dot_general | solution.py:505
  6.8 0.1 copy.65
  6.9 0.7 add_divide_fusion.b
  7.7 0.3 fusion.4
  7.9 0.8 copy.69.g
  8.8 0.6 reshape.121.row
  9.4 0.4 copy.90
  9.8 1.2 reshape.123.hid
  11.0 47.2 %front.1 = (bf16[8,256,256]{2,1,0:T(8,128)(2,1)}, f32[8,256,256]{2,1,0:T(8,128)}, f32[8,256,128]{2,1,0:T(8,128)}, bf16[8,128,128]{2,1,0:T(8,128)(2,1)}, bf16[8,1...) custom-call(bf16[256,1024]{1,0:T(8,128)(2,1)} %q.3, bf16[256,1024]{1,0:T(8,128)(2,1)} %k.5, ...), custom_call_target="tpu_custom_call" | custom-call | flops 1073741824 | bytes 8388608 | tf_op jit(solution)/shard_map/front/pallas_call | solution.py:525
  58.2 4.7 %value.1 = (f32[8,256,128]{2,1,0:T(8,128)}, bf16[256,1024]{1,0:T(8,128)(2,1)}) custom-call(bf16[256,1024]{1,0:T(8,128)(2,1)} %k.5, bf16[8,256,256]{2,1,0:T(8,128)(2,1)} %get-tuple-element.24.inv, f32[8,256,128]{2,1,0:T(8,128)} %get-tuple-element.25.dw, bf16[8,128,128]{2,1,0:T(8,128)(2,1)} %get-tuple-element.26.end, f32[256,8]{1,0:T(8,128)} %add_divide_fusion.b, ...), custom_call_target="tpu_custom_call" | custom-call | tf_op jit(solution)/shard_map/value/pallas_call | solution.py:549
  62.9 4.6 %convolution_convert_fusion = bf16[128,2048]{1,0:T(8,128)(2,1)} fusion(bf16[2048,1024]{1,0:T(8,128)(2,1)} %param.11, bf16[256,1024]{1,0:T(8,128)(2,1)} %get-tuple-element.27, s32[]{:T(128)S(6)} %select_n.71), kind=kOutput, calls=%fused_computation | convolution fusion | flops 537133056 | bytes 4980740 | tf_op jit(solution)/shard_map/dot_general | solution.py:489
  67.5 0.0 collective-permute-start
  67.5 0.5 copy.70
  68.0 0.0 copy-start
  68.0 0.1 constant_dynamic-slice_fusion.2
  68.1 0.9 copy-done
  69.0 1.3 convolution_convert_fusion.3
  70.4 0.1 constant_dynamic-slice_fusion.1
  70.4 1.3 convolution_convert_fusion.2
  71.8 0.1 constant_dynamic-slice_fusion
  71.9 1.1 convolution_convert_fusion.4
  73.0 0.0 collective-permute-start.9
  73.0 0.3 collective-permute-start.5
  73.3 1.1 collective-permute-start.1
  74.4 9.8 %last.1 = (bf16[256,1024]{1,0:T(8,128)(2,1)}, bf16[256,1024]{1,0:T(8,128)(2,1)}, f32[256,8]{1,0:T(8,128)}, f32[256,8]{1,0:T(8,128)}, f32[8,1,256]{2,1,0:T(1,128)}) custom-call(bf16[256,1024]{1,0:T(8,128)(2,1)} %q.3, bf16[256,1024]{1,0:T(8,128)(2,1)} %k.5, bf16[256,1024]{1,0:T(8,128)(2,1)} %convolution_convert_fusion.5.v, bf16[256,1024]{1,0:T(8,128)(2,1)} %do.3, ...), custom_call_target="tpu_custom_call" | custom-call | flops 1744830464 | bytes 12582912 | tf_op jit(solution)/shard_map/last/pallas_call | solution.py:567
  84.3 1.0 subtract_multiply_fusion
  85.2 0.7 copy.79
  85.9 1.0 copy.74
  86.8 1.5 %convolution_multiply_fusion = f32[256,8]{0,1:T(8,128)} fusion(f32[256,8]{0,1:T(8,128)S(1)} %copy.74, f32[8,1,256]{2,1,0:T(1,128)} %get-tuple-element.36, f32[256,8]{0,1:T(8,128)S(1)} %copy-done.3, f32[8]{0:T(128)S(1)} %neg.16), kind=kOutput, calls=%fused_computation.9 | convolution fusion | flops 6434816 | bytes 32800 | tf_op jit(solution)/shard_map/dot_general | solution.py:587
  88.4 0.0 collective-permute-done.9
  88.4 1.3 convert_add_fusion.2
  89.8 3.3 %collective-permute-start.10 = (bf16[1,512,256]{2,1,0:T(8,128)(2,1)S(1)}, bf16[1,512,256]{2,1,0:T(8,128)(2,1)S(1)}, u32[]{:S(2)}, u32[]{:S(2)}) collective-permute-start(bf16[1,512,256]{2,1,0:T(8,128)(2,1)S(1)} %fusion.6), channel_id=1, source_target_pairs={{0,16},{2,18},{4,20},{6,22},{8,24},{10,26},{12,28},{14,30},{16,0},... | collective-permute-start | bytes 786440 | tf_op jit(solution)/shard_map/ppermute | solution.py:428
  93.1 0.0 collective-permute-done
  93.1 4.6 %add_convert_fusion = bf16[128,2048]{1,0:T(8,128)(2,1)} fusion(bf16[128,2048]{1,0:T(8,128)(2,1)} %collective-permute-done, bf16[2048,1024]{1,0:T(8,128)(2,1)} %param.11, bf16[256,1024]{1,0:T(8,128)(2,1)S(1)} %copy-done, s32[]{:T(128)S(6)} %select_n.70), kind=kOutput, calls=%fused_computation.12 | convolution fusion | flops 538181632 | bytes 5505028 | tf_op jit(solution)/shard_map/dot_general | solution.py:489
  97.7 7.1 %collective-permute-done.10 = bf16[1,512,256]{2,1,0:T(8,128)(2,1)S(1)} collective-permute-done((bf16[1,512,256]{2,1,0:T(8,128)(2,1)S(1)}, bf16[1,512,256]{2,1,0:T(8,128)(2,1)S(1)}, u32[]{:S(2)}, u32[]{:S(2)}) %collective-permute-start.10) | collective-permute-done | bytes 262176 | tf_op jit(solution)/shard_map/ppermute | solution.py:428
  104.8 0.1 bitcast_add_fusion.2
  104.9 1.0 collective-permute-start.11
  105.9 0.0 collective-permute-done.5
  105.9 1.6 %convert_add_fusion = f32[1024,384]{1,0:T(8,128)S(1)} fusion(bf16[1024,384]{1,0:T(8,128)(2,1)} %collective-permute-done.5, bf16[256,1024]{0,1:T(8,128)(2,1)S(1)} %bitcast.97, bf16[256,1024]{1,0:T(8,128)(2,1)S(1)} %copy-done), kind=kOutput, calls=%fused_computation.3 | convolution fusion | flops 202113024 | bytes 3080192 | tf_op jit(solution)/shard_map/dot_general | solution.py:448
  107.5 0.1 fusion.1
  107.6 1.1 collective-permute-start.6
  108.7 0.0 collective-permute-done.1
  108.7 0.4 convert_add_fusion.1
  109.1 1.7 %collective-permute-done.11 = bf16[2,128,256]{2,1,0:T(8,128)(2,1)S(1)} collective-permute-done((bf16[2,128,256]{2,1,0:T(8,128)(2,1)S(1)}, bf16[2,128,256]{2,1,0:T(8,128)(2,1)S(1)}, u32[]{:S(2)}, u32[]{:S(2)}) %collective-permute-start.11) | collective-permute-done | bytes 131104 | tf_op jit(solution)/shard_map/ppermute | solution.py:428
  110.8 0.9 collective-permute-start.12
  111.8 1.2 collective-permute-start.2
  113.1 2.8 %collective-permute-done.12 = bf16[1,128,256]{2,1,0:T(8,128)(2,1)S(1)} collective-permute-done((bf16[1,128,256]{2,1,0:T(8,128)(2,1)S(1)}, bf16[1,128,256]{2,1,0:T(8,128)(2,1)S(1)}, u32[]{:S(2)}, u32[]{:S(2)}) %collective-permute-start.12) | collective-permute-done | bytes 65568 | tf_op jit(solution)/shard_map/ppermute | solution.py:428
  115.9 2.5 %collective-permute-done.6 = bf16[4,128,384]{2,1,0:T(8,128)(2,1)S(1)} collective-permute-done((bf16[4,128,384]{2,1,0:T(8,128)(2,1)S(1)}, bf16[4,128,384]{2,1,0:T(8,128)(2,1)S(1)}, u32[]{:S(2)}, u32[]{:S(2)}) %collective-permute-start.6) | collective-permute-done | bytes 393248 | tf_op jit(solution)/shard_map/ppermute | solution.py:428
  118.4 0.1 bitcast_add_fusion
  118.5 0.1 collective-permute-start.7
  118.6 2.1 %collective-permute-done.2 = bf16[4,128,384]{2,1,0:T(8,128)(2,1)S(1)} collective-permute-done((bf16[4,128,384]{2,1,0:T(8,128)(2,1)S(1)}, bf16[4,128,384]{2,1,0:T(8,128)(2,1)S(1)}, u32[]{:S(2)}, u32[]{:S(2)}) %collective-permute-start.2) | collective-permute-done | bytes 393248 | tf_op jit(solution)/shard_map/ppermute | solution.py:428
  120.6 0.1 bitcast_add_fusion.1
  120.7 0.1 collective-permute-start.3
  120.8 6.6 %collective-permute-done.7 = bf16[2,128,384]{2,1,0:T(8,128)(2,1)S(1)} collective-permute-done((bf16[2,128,384]{2,1,0:T(8,128)(2,1)S(1)}, bf16[2,128,384]{2,1,0:T(8,128)(2,1)S(1)}, u32[]{:S(2)}, u32[]{:S(2)}) %collective-permute-start.7) | collective-permute-done | bytes 196640 | tf_op jit(solution)/shard_map/ppermute | solution.py:428
  127.5 0.5 collective-permute-start.8
  128.0 1.5 %collective-permute-done.3 = bf16[2,128,384]{2,1,0:T(8,128)(2,1)S(1)} collective-permute-done((bf16[2,128,384]{2,1,0:T(8,128)(2,1)S(1)}, bf16[2,128,384]{2,1,0:T(8,128)(2,1)S(1)}, u32[]{:S(2)}, u32[]{:S(2)}) %collective-permute-start.3) | collective-permute-done | bytes 196640 | tf_op jit(solution)/shard_map/ppermute | solution.py:428
  129.6 1.2 collective-permute-start.4
  130.8 5.3 %collective-permute-done.8 = bf16[1,128,384]{2,1,0:T(8,128)(2,1)S(1)} collective-permute-done((bf16[1,128,384]{2,1,0:T(8,128)(2,1)S(1)}, bf16[1,128,384]{2,1,0:T(8,128)(2,1)S(1)}, u32[]{:S(2)}, u32[]{:S(2)}) %collective-permute-start.8) | collective-permute-done | bytes 98336 | tf_op jit(solution)/shard_map/ppermute | solution.py:428
  136.1 1.0 collective-permute-done.4
  137.2 0.8 pad_maximum_fusion
  (20 shorter events, 0.4 us)
Async XLA Ops:
  0.6 1.9 %copy-start.1 = (bf16[256,2048]{1,0:T(8,128)(2,1)S(1)}, bf16[256,2048]{1,0:T(8,128)(2,1)}, u32[]{:S(2)}) copy-start(bf16[256,2048]{1,0:T(8,128)(2,1)} %param.10) | copy-start | bytes 3145732
  2.5 4.3 %copy-start.2 = (f32[256,8]{0,1:T(8,128)S(1)}, f32[256,8]{0,1:T(8,128)}, u32[]{:S(2)}) copy-start(f32[256,8]{0,1:T(8,128)} %param.12) | copy-start | bytes 24580
  2.5 5.1 %copy-start.4 = (f32[8]{0:T(128)S(1)}, f32[8]{0:T(128)}, u32[]{:S(2)}) copy-start(f32[8]{0:T(128)} %param.14) | copy-start | bytes 100
  2.6 5.1 %copy-start.3 = (f32[256,8]{0,1:T(8,128)S(1)}, f32[256,8]{0,1:T(8,128)}, u32[]{:S(2)}) copy-start(f32[256,8]{0,1:T(8,128)} %param.13) | copy-start | bytes 24580
  67.5 25.6 %collective-permute-start = (bf16[128,2048]{1,0:T(8,128)(2,1)}, bf16[128,2048]{1,0:T(8,128)(2,1)}, u32[]{:S(2)}, u32[]{:S(2)}) collective-permute-start(bf16[128,2048]{1,0:T(8,128)(2,1)} %convolution_convert_fusion), channel_id=1, source_target_pairs={{0,1},{1,0},{2,3},{3,2},{4,5},{5,4},{6,7},{7,6},{8,9},{9,8},{10,11... | collective-permute-start | bytes 1572872 | tf_op jit(solution)/shard_map/ppermute | solution.py:428
  68.0 1.0 copy-start
  73.0 15.4 %collective-permute-start.9 = (bf16[1024,256]{1,0:T(8,128)(2,1)}, bf16[1024,256]{1,0:T(8,128)(2,1)}, u32[]{:S(2)}, u32[]{:S(2)}) collective-permute-start(bf16[1024,256]{1,0:T(8,128)(2,1)} %convolution_convert_fusion.4), channel_id=1, source_target_pairs={{0,8},{2,10},{4,12},{6,14},{8,0},{10,2},{12,4},{14,6},{16,24},{18,... | collective-permute-start | bytes 1572872 | tf_op jit(solution)/shard_map/ppermute | solution.py:428
  73.0 33.0 %collective-permute-start.5 = (bf16[1024,384]{1,0:T(8,128)(2,1)}, bf16[1024,384]{1,0:T(8,128)(2,1)}, u32[]{:S(2)}, u32[]{:S(2)}) collective-permute-start(bf16[1024,384]{1,0:T(8,128)(2,1)} %convolution_convert_fusion.2), channel_id=1, source_target_pairs={{0,4},{2,6},{4,0},{6,2},{8,12},{10,14},{12,8},{14,10},{16,20},{18,... | collective-permute-start | bytes 2359304 | tf_op jit(solution)/shard_map/ppermute | solution.py:428
  73.3 35.4 %collective-permute-start.1 = (bf16[1024,384]{1,0:T(8,128)(2,1)}, bf16[1024,384]{1,0:T(8,128)(2,1)S(1)}, u32[]{:S(2)}, u32[]{:S(2)}) collective-permute-start(bf16[1024,384]{1,0:T(8,128)(2,1)} %convolution_convert_fusion.3), channel_id=1, source_target_pairs={{0,2},{2,0},{4,6},{6,4},{8,10},{10,8},{12,14},{14,12},{16,18},{18,... | collective-permute-start | bytes 2359304 | tf_op jit(solution)/shard_map/ppermute | solution.py:428
  89.8 15.1 %collective-permute-start.10 = (bf16[1,512,256]{2,1,0:T(8,128)(2,1)S(1)}, bf16[1,512,256]{2,1,0:T(8,128)(2,1)S(1)}, u32[]{:S(2)}, u32[]{:S(2)}) collective-permute-start(bf16[1,512,256]{2,1,0:T(8,128)(2,1)S(1)} %fusion.6), channel_id=1, source_target_pairs={{0,16},{2,18},{4,20},{6,22},{8,24},{10,26},{12,28},{14,30},{16,0},... | collective-permute-start | bytes 786440 | tf_op jit(solution)/shard_map/ppermute | solution.py:428
  104.9 5.9 %collective-permute-start.11 = (bf16[2,128,256]{2,1,0:T(8,128)(2,1)S(1)}, bf16[2,128,256]{2,1,0:T(8,128)(2,1)S(1)}, u32[]{:S(2)}, u32[]{:S(2)}) collective-permute-start(bf16[2,128,256]{2,1,0:T(8,128)(2,1)S(1)} %fusion.23), channel_id=1, source_target_pairs={{0,2},{2,0},{4,6},{6,4},{8,10},{10,8},{12,14},{14,12},{16,18},{18,... | collective-permute-start | bytes 393224 | tf_op jit(solution)/shard_map/ppermute | solution.py:428
  107.6 10.8 %collective-permute-start.6 = (bf16[4,128,384]{2,1,0:T(8,128)(2,1)S(1)}, bf16[4,128,384]{2,1,0:T(8,128)(2,1)S(1)}, u32[]{:S(2)}, u32[]{:S(2)}) collective-permute-start(bf16[4,128,384]{2,1,0:T(8,128)(2,1)S(1)} %fusion.1), channel_id=1, source_target_pairs={{0,2},{2,0},{4,6},{6,4},{8,10},{10,8},{12,14},{14,12},{16,18},{18,... | collective-permute-start | bytes 1179656 | tf_op jit(solution)/shard_map/ppermute | solution.py:428
  110.8 5.0 %collective-permute-start.12 = (bf16[1,128,256]{2,1,0:T(8,128)(2,1)S(1)}, bf16[1,128,256]{2,1,0:T(8,128)(2,1)S(1)}, u32[]{:S(2)}, u32[]{:S(2)}) collective-permute-start(bf16[1,128,256]{2,1,0:T(8,128)(2,1)S(1)} %dynamic-slice_convert_fusion.4), channel_id=1, source_target_pairs={{0,4},{2,6},{4,0},{6,2},{8,12},{10,14},{12,8},{14,10},{16,20},{18,... | collective-permute-start | bytes 196616 | tf_op jit(solution)/shard_map/ppermute | solution.py:428
  111.8 8.8 %collective-permute-start.2 = (bf16[4,128,384]{2,1,0:T(8,128)(2,1)S(1)}, bf16[4,128,384]{2,1,0:T(8,128)(2,1)S(1)}, u32[]{:S(2)}, u32[]{:S(2)}) collective-permute-start(bf16[4,128,384]{2,1,0:T(8,128)(2,1)S(1)} %fusion.2), channel_id=1, source_target_pairs={{0,4},{2,6},{4,0},{6,2},{8,12},{10,14},{12,8},{14,10},{16,20},{18,... | collective-permute-start | bytes 1179656 | tf_op jit(solution)/shard_map/ppermute | solution.py:428
  118.5 8.9 %collective-permute-start.7 = (bf16[2,128,384]{2,1,0:T(8,128)(2,1)S(1)}, bf16[2,128,384]{2,1,0:T(8,128)(2,1)S(1)}, u32[]{:S(2)}, u32[]{:S(2)}) collective-permute-start(bf16[2,128,384]{2,1,0:T(8,128)(2,1)S(1)} %fusion.12), channel_id=1, source_target_pairs={{0,8},{2,10},{4,12},{6,14},{8,0},{10,2},{12,4},{14,6},{16,24},{18,... | collective-permute-start | bytes 589832 | tf_op jit(solution)/shard_map/ppermute | solution.py:428
  120.7 8.8 %collective-permute-start.3 = (bf16[2,128,384]{2,1,0:T(8,128)(2,1)S(1)}, bf16[2,128,384]{2,1,0:T(8,128)(2,1)S(1)}, u32[]{:S(2)}, u32[]{:S(2)}) collective-permute-start(bf16[2,128,384]{2,1,0:T(8,128)(2,1)S(1)} %fusion.11), channel_id=1, source_target_pairs={{0,8},{2,10},{4,12},{6,14},{8,0},{10,2},{12,4},{14,6},{16,24},{18,... | collective-permute-start | bytes 589832 | tf_op jit(solution)/shard_map/ppermute | solution.py:428
  127.5 8.6 %collective-permute-start.8 = (bf16[1,128,384]{2,1,0:T(8,128)(2,1)S(1)}, bf16[1,128,384]{2,1,0:T(8,128)(2,1)S(1)}, u32[]{:S(2)}, u32[]{:S(2)}) collective-permute-start(bf16[1,128,384]{2,1,0:T(8,128)(2,1)S(1)} %dynamic-slice_convert_fusion.2), channel_id=1, source_target_pairs={{0,16},{2,18},{4,20},{6,22},{8,24},{10,26},{12,28},{14,30},{16,0},... | collective-permute-start | bytes 294920 | tf_op jit(solution)/shard_map/ppermute | solution.py:428
  129.6 7.6 %collective-permute-start.4 = (bf16[1,128,384]{2,1,0:T(8,128)(2,1)S(1)}, bf16[1,128,384]{2,1,0:T(8,128)(2,1)S(1)}, u32[]{:S(2)}, u32[]{:S(2)}) collective-permute-start(bf16[1,128,384]{2,1,0:T(8,128)(2,1)S(1)} %dynamic-slice_convert_fusion.3), channel_id=1, source_target_pairs={{0,16},{2,18},{4,20},{6,22},{8,24},{10,26},{12,28},{14,30},{16,0},... | collective-permute-start | bytes 294920 | tf_op jit(solution)/shard_map/ppermute | solution.py:428
where the time goes:
time: 138 us
  Pallas kernels  61.7 us (45%)
  waiting for transfers between devices  30.5 us (22%)
  matrix products  22.3 us (16%)
  starting transfers between devices  10.9 us (8%)
  local copies, waits for them, and re-layouts  8.7 us (6%)
  other arithmetic  2.85 us (2%)
    pallas_call x1, Pallas kernels, compute(): pl.pallas_call(functools.partial(front_kernel, count), in_specs=[vmem] *...  47.2 us
    ppermute x13, waiting for transfers between devices, exchange(): return lax.ppermute(value, axis, [(i, i ^ bit) for i in range(count)])  30.5 us
    ppermute x13, starting transfers between devices, exchange(): return lax.ppermute(value, axis, [(i, i ^ bit) for i in range(count)])  10.9 us
    pallas_call x1, Pallas kernels, compute(): pl.pallas_call(functools.partial(last_kernel, group), grid=(heads // grou...  9.85 us
    dot_general x2, matrix products, product(): lax.dot_general(rows, weight, (((1,), (1,)), ((), ())), preferred_element...  9.2 us
    dot_general x6, matrix products, product(): lax.dot_general(piece, self.grads, (((0,), (0,)), ((), ())), preferred_el...  7.09 us
    pallas_call x1, Pallas kernels, compute(): pl.pallas_call(functools.partial(value_kernel, group), grid=(heads // gro...  4.68 us
    dot_general x1, matrix products, compute(): jnp.dot(hidden, value_weight, preferred_element_type=f32).astype(bf16)  4.24 us
  transfers between devices with their start and end apart: 13, of which 9 were waited for; matrix products, arithmetic and copies ran while one was open for 12% of the time, Pallas kernels for 7%

commit v1 on v0

--- a/solution.py
+++ b/solution.py
@@ -6,7 +6,6 @@
 from jax.experimental import pallas as pl
 from jax.experimental.pallas import tpu as pltpu
 from jax.sharding import PartitionSpec as P
-
 
 f32 = jnp.float32
 bf16 = jnp.bfloat16
@@ -183,11 +182,6 @@
     return pick(g_ref, head), gr, gr[:, gr.shape[1] - 1 :]
 
 
-def lanes(ref, i, group):
-    width = ref.shape[1] // group
-    return ref.at[:, i * width : (i + 1) * width]
-
-
 PEERS = 4
 MESH = pl.DeviceIdType.MESH
 
@@ -393,106 +387,225 @@
             chain_copy(1, i).wait_send()
 
 
-def value_kernel(group, k, inv, dw, end, b, g, row, dr_o, dv_o):
-    for i in range(group):
-        head = pl.program_id(0) * group + i
-        gc, _, ge = gains(g, row.at[i], head)
-        bc = pick(b, head)
-        dr = value_phase(lanes(k, i, group)[...].astype(f32), inv[i], dw[i], end[i], gc, ge)
-        dr_o[i] = dr
-        lanes(dv_o, i, group)[...] = (bc * dr).astype(bf16)
-
-
-def last_kernel(group, q, k, v, do, uw, dr, start, end, b, g, row, dq_o, dk_o, db_o, gc_o, gr_o):
-    @pl.when(pl.program_id(0) == 0)
-    def _():
-        db_o[...] = jnp.zeros_like(db_o)
-        gc_o[...] = jnp.zeros_like(gc_o)
-
-    for i in range(group):
-        head = pl.program_id(0) * group + i
-        gc, gr, ge = gains(g, row.at[i], head)
-        raw = [lanes(a, i, group)[...].astype(f32) for a in (q, k, v, do)]
+def back_kernel(
+    count, q, k, v, do, uw, inv, dw, start, end, b, g, row, hid, w,
+    dq_o, dk_o, db_o, gc_o, gr_o, dh_o, dwt_o,
+    dr_s, grads, turned, prod, up_out, up_in, down_out, down_in, share_out, share_in,
+    near_send, near_recv, far_send, far_recv, up_send, up_recv, down_send, down_recv, share_sems,
+):
+    at = Place(count)
+    heads = row.shape[0]
+    own = heads // PEERS
+    length = q.shape[0]
+    dk = q.shape[1] // heads
+    dv = v.shape[1] // heads
+    wide = own * dv
+    chain = at.chain
+    rows = hid.shape[2] // chain
+    half = length // 2
+    me = lax.axis_index("sp")
+    twin = (me, 1 - at.core)
+    at.greet([at.at_peer(1), at.at_peer(2), twin] + at.ring())
+
+    def near(c, j):
+        return remote(grads.at[0, c], grads.at[j, c], near_send.at[j - 1, c], near_recv.at[j - 1, c], at.at_peer(j))
+
+    def far(c, j):
+        piece = pl.ds((2 - j) * half, half)
+        return remote(
+            grads.at[3 - j, c, piece], grads.at[3, c, piece],
+            far_send.at[j - 1, c], far_recv.at[j - 1, c], at.at_peer(j),
+        )
+
+    def values(c, carry):
+        for i in range(own):
+            head = c * own + i
+            gc, _, ge = gains(g, row.at[head], head)
+            bc = pick(b, head)
+            dr = value_phase(head_lanes(k, head, dk)[...].astype(f32), inv[head], dw[head], end[head], gc, ge)
+            dr_s[head] = dr
+            grads[0, c, :, i * dv : (i + 1) * dv] = (bc * dr).astype(bf16)
+        near(c, 1).start()
+        near(c, 2).start()
+        return carry
+
+    lax.fori_loop(0, PEERS, values, 0)
+    for j in range(PEERS):
+        turned[j] = hid[j].T
+
+    db_o[...] = jnp.zeros_like(db_o)
+    gc_o[...] = jnp.zeros_like(gc_o)
+
+    def last_head(head):
+        gc, gr, ge = gains(g, row.at[head], head)
+        raw = [head_lanes(a, head, dk)[...].astype(f32) for a in (q, k)]
+        raw += [head_lanes(a, head, dv)[...].astype(f32) for a in (v, do)]
         dqr, dkr, db, gcol, grow = last_phase(
-            *raw, uw[i], dr[i], start[i].astype(f32), end[i].astype(f32), pick(b, head), gc, gr, ge
+            *raw, uw[head], dr_s[head], start[head].astype(f32), end[head].astype(f32), pick(b, head), gc, gr, ge
         )
-        lanes(dq_o, i, group)[...] = dqr.astype(bf16)
-        lanes(dk_o, i, group)[...] = dkr.astype(bf16)
+        head_lanes(dq_o, head, dk)[...] = dqr.astype(bf16)
+        head_lanes(dk_o, head, dk)[...] = dkr.astype(bf16)
         put(db_o, head, db)
         put(gc_o, head, gcol)
-        gr_o[i] = grow
-
-
-def exchange(value, axis, bit):
-    count = lax.axis_size(axis)
-    return lax.ppermute(value, axis, [(i, i ^ bit) for i in range(count)])
-
-
-def bit_of(axis, bit):
-    return (lax.axis_index(axis) >> bit) & 1
-
-
-class Halving:
-    def __init__(self, hidden, grads, bits, sequence):
-        self.grads, self.sequence = grads, sequence
-        self.length, self.rows, self.count = hidden.shape[0], hidden.shape[1], 1 << bits
-        self.left = sorted(range(bits), reverse=True)
-        self.axis = 1 + self.left.index(sequence[0])
-        self.mine = bit_of("sp", sequence[0])
-        self.split = hidden.reshape((self.length,) + (2,) * bits + (self.rows // self.count,))
-        self.send = self.product(1 - self.mine).astype(bf16)
-
-    def product(self, side):
-        piece = lax.dynamic_index_in_dim(self.split, side, self.axis, False)
-        piece = piece.reshape(self.length, self.rows // 2)
-        return lax.dot_general(
-            piece, self.grads, (((0,), (0,)), ((), ())), preferred_element_type=f32
+        gr_o[head] = grow
+
+    def forward(c):
+        near(c, 1).wait_recv()
+        far(c, 2).start()
+        near(c, 2).wait_recv()
+        far(c, 1).start()
+
+    def up(c, d):
+        return remote(
+            up_out.at[c, d], up_in.at[c, d], up_send.at[c, d], up_recv.at[c, d], at.at_group((at.q + 1) % chain)
         )
 
-    def finish(self, send):
-        left = list(self.left)
-        got = exchange(send, "sp", 1 << self.sequence[0])
-        total = self.product(self.mine) + got.astype(f32)
-        left.remove(self.sequence[0])
-        for bit in self.sequence[1:]:
-            place = left.index(bit)
-            mine = bit_of("sp", bit)
-            shaped = total.reshape(1 << place, 2, -1, total.shape[-1])
-            send = lax.dynamic_index_in_dim(shaped, 1 - mine, 1, False)
-            keep = lax.dynamic_index_in_dim(shaped, mine, 1, False)
-            got = exchange(send.astype(bf16), "sp", 1 << bit)
-            total = keep + got.astype(f32)
-            left.remove(bit)
-        return total.reshape(self.rows // self.count, -1)
-
-
-def plan_weight(hidden, grads, count):
-    bits = count.bit_length() - 1
-    low = bits // 2
-    order_a = list(range(bits))
-    order_b = order_a[:low][::-1] + order_a[low:]
-    order_c = order_a[low:] + order_a[:low]
-    width = grads.shape[1]
-    cut = max(width * 3 // 8 // 128 * 128, 1)
-    groups = [(0, cut, order_a), (cut, 2 * cut, order_b), (2 * cut, width, order_c)]
-    return [Halving(hidden, grads[:, lo:hi], bits, seq) for lo, hi, seq in groups]
-
-
-def reduce_hidden(grads, weight):
-    cores = lax.axis_size("tp")
-    assert cores == 2
-    half = grads.shape[0] // cores
-    me = lax.axis_index("tp")
-
-    def product(side):
-        rows = lax.dynamic_slice_in_dim(grads, side * half, half, 0)
-        return lax.dot_general(
-            rows, weight, (((1,), (1,)), ((), ())), preferred_element_type=f32
-        ).astype(bf16)
-
-    send = product(1 - me)
-    got = exchange(send, "tp", 1)
-    return (product(me).astype(f32) + got.astype(f32)).astype(bf16)
+    def down(c, d):
+        return remote(
+            down_out.at[c, d], down_in.at[c, d], down_send.at[c, d], down_recv.at[c, d],
+            at.at_group((at.q + chain - 1) % chain),
+        )
+
+    def product(c):
+        far(c, 1).wait_recv()
+        far(c, 2).wait_recv()
+        total = nn(turned[0], grads[0, c])
+        for j in range(1, PEERS):
+            total = total + nn(turned[j], grads[j, c])
+        prod[c] = total.reshape(chain, rows, wide)
+
+        @pl.when(at.q == 0)
+        def _():
+            def send(n, carry):
+                d = chain - 1 - n
+                up_out[c, d] = prod[c, d].astype(bf16)
+                up(c, d).start()
+                return carry
+
+            lax.fori_loop(0, chain - 1, send, 0)
+
+        @pl.when(at.q == chain - 1)
+        def _():
+            def send(d, carry):
+                down_out[c, d] = prod[c, d].astype(bf16)
+                down(c, d).start()
+                return carry
+
+            lax.fori_loop(0, chain - 1, send, 0)
+
+    def pass_up(c):
+        def step(n, carry):
+            d = chain - 1 - n
+
+            @pl.when(d > at.q)
+            def _():
+                up(c, d).wait_recv()
+                up_out[c, d] = (prod[c, d] + up_in[c, d].astype(f32)).astype(bf16)
+                up(c, d).start()
+
+            return carry
+
+        lax.fori_loop(0, chain - 1, step, 0)
+
+    def pass_down(c):
+        def step(d, carry):
+            @pl.when(d < at.q)
+            def _():
+                down(c, d).wait_recv()
+                down_out[c, d] = (prod[c, d] + down_in[c, d].astype(f32)).astype(bf16)
+                down(c, d).start()
+
+            return carry
+
+        lax.fori_loop(0, chain - 1, step, 0)
+
+    def relay(c):
+        low = at.q < chain // 2
+
+        @pl.when((at.q > 0) & low)
+        def _():
+            pass_up(c)
+
+        @pl.when((at.q > 0) & (at.q < chain - 1))
+        def _():
+            pass_down(c)
+
+        @pl.when((at.q < chain - 1) & (at.q >= chain // 2))
+        def _():
+            pass_up(c)
+
+    def finish(c):
+        total = prod[c, at.q]
+        prod[c, at.q] = total
+
+        @pl.when(at.q > 0)
+        def _():
+            up(c, at.q).wait_recv()
+            prod[c, at.q] = prod[c, at.q] + up_in[c, at.q].astype(f32)
+
+        @pl.when(at.q < chain - 1)
+        def _():
+            down(c, at.q).wait_recv()
+            prod[c, at.q] = prod[c, at.q] + down_in[c, at.q].astype(f32)
+
+        dwt_o[:, pl.ds(pl.multiple_of(c * wide, wide), wide)] = prod[c, at.q]
+
+    share = remote(share_out, share_in, share_sems.at[0], share_sems.at[1], twin)
+
+    def hidden_half(side):
+        total = 0
+        for c in range(PEERS):
+            piece = grads[0, c, pl.ds(pl.multiple_of(side * half, half), half)]
+            total = total + nt(piece, w[:, c * wide : (c + 1) * wide])
+        return total
+
+    def step(c, carry):
+        @pl.when(c < PEERS)
+        def _():
+            for i in range(own):
+                last_head(c * own + i)
+            forward(c)
+
+        @pl.when(c > 0)
+        def _():
+            product(c - 1)
+
+        @pl.when(c > 1)
+        def _():
+            relay(c - 2)
+
+        return carry
+
+    lax.fori_loop(0, PEERS + 1, step, 0)
+    share_out[...] = hidden_half(1 - at.core).astype(bf16)
+    share.start()
+    relay(PEERS - 1)
+    mine = hidden_half(at.core).astype(bf16).astype(f32)
+    share.wait_recv()
+    dh_o[...] = (mine + share_in[...].astype(f32)).astype(bf16)
+    share.wait_send()
+
+    def close(c, carry):
+        finish(c)
+        for j in (1, 2):
+            near(c, j).wait_send()
+            far(c, j).wait_send()
+
+        def sent(d, inner):
+            @pl.when(d > at.q)
+            def _():
+                up(c, d).wait_send()
+
+            @pl.when(d < at.q)
+            def _():
+                down(c, d).wait_send()
+
+            return inner
+
+        lax.fori_loop(0, chain, sent, 0)
+        return carry
+
+    lax.fori_loop(0, PEERS, close, 0)
 
 
 def compute(queries, keys, hidden, value_weight, beta_pre, decay_pre, decay_rate, out_grad):
@@ -500,7 +613,6 @@
     length, dk = queries.shape[0], queries.shape[1] // heads
     dv = value_weight.shape[1] // heads
     count = lax.axis_size("sp")
-    group = 4 if heads % 4 == 0 else 1
 
     values = jnp.dot(hidden, value_weight, preferred_element_type=f32).astype(bf16)
     beta = jax.nn.sigmoid(beta_pre)
@@ -509,12 +621,7 @@
     sums = jnp.dot(inclusive, log_decay, precision=lax.Precision.HIGHEST)
     sums_row = sums.T.reshape(heads, 1, length)
 
-    wide = lambda n: pl.BlockSpec((length, group * n), lambda h: (0, h))
-    per_head = lambda r, c: pl.BlockSpec((group, r, c), lambda h: (h, 0, 0))
-    table = pl.BlockSpec((length, heads), lambda h: (0, 0))
     shape = jax.ShapeDtypeStruct
-    params = pltpu.CompilerParams(dimension_semantics=("arbitrary",))
-
     own = heads // PEERS
     chain = count // PEERS
     rows = hidden.shape[1] // count
@@ -522,7 +629,7 @@
     pieces = jnp.moveaxis(pieces, 2, 0).reshape(PEERS, length, chain * rows)
     vmem = pl.BlockSpec(memory_space=pltpu.VMEM)
     dma = pltpu.SemaphoreType.DMA
-    inverse, uw, dw0, start, end, _ = pl.pallas_call(
+    inverse, uw, dw0, start, end, hidden_all = pl.pallas_call(
         functools.partial(front_kernel, count),
         in_specs=[vmem] * 8,
         out_specs=[vmem] * 6,
@@ -546,43 +653,34 @@
         name="front",
     )(queries, keys, values, out_grad, beta, sums, sums_row, pieces)
 
-    dr, grad_values = pl.pallas_call(
-        functools.partial(value_kernel, group),
-        grid=(heads // group,),
-        in_specs=[
-            wide(dk), per_head(length, length), per_head(length, dv), per_head(dk, dv),
-            table, table, per_head(1, length),
-        ],
-        out_specs=[per_head(length, dv), wide(dv)],
-        out_shape=[shape((heads, length, dv), f32), shape((length, heads * dv), bf16)],
-        compiler_params=params,
-        name="value",
-    )(keys, inverse, dw0, end, beta, sums, sums_row)
-
-    plans = plan_weight(hidden, grad_values, count)
-    sends, dr, start = lax.optimization_barrier(([plan.send for plan in plans], dr, start))
-    d_weight = jnp.concatenate([plan.finish(x) for plan, x in zip(plans, sends)], axis=1)
-    d_hidden = reduce_hidden(grad_values, value_weight)
-
-    d_queries, d_keys, db, gcol, grow = pl.pallas_call(
-        functools.partial(last_kernel, group),
-        grid=(heads // group,),
-        in_specs=[
-            wide(dk), wide(dk), wide(dv), wide(dv), per_head(length, dv + dk),
-            per_head(length, dv), per_head(dk, dv), per_head(dk, dv),
-            table, table, per_head(1, length),
-        ],
-        out_specs=[wide(dk), wide(dk), table, table, per_head(1, length)],
+    wide = own * dv
+    d_queries, d_keys, db, gcol, grow, d_hidden, d_weight = pl.pallas_call(
+        functools.partial(back_kernel, count),
+        in_specs=[vmem] * 14,
+        out_specs=[vmem] * 7,
         out_shape=[
             shape(queries.shape, bf16), shape(keys.shape, bf16), shape((length, heads), f32),
             shape((length, heads), f32), shape((heads, 1, length), f32),
+            shape((length // 2, hidden.shape[1]), bf16), shape((rows, heads * dv), f32),
         ],
-        compiler_params=params,
-        cost_estimate=pl.CostEstimate(
-            flops=heads * 13 * 2 * length * length * dk, bytes_accessed=12 << 20, transcendentals=0
-        ),
-        name="last",
-    )(queries, keys, values, out_grad, uw, dr, start, end, beta, sums, sums_row)
+        scratch_shapes=[
+            pltpu.VMEM((heads, length, dv), f32),
+            pltpu.VMEM((PEERS, PEERS, length, wide), bf16),
+            pltpu.VMEM((PEERS, chain * rows, length), bf16),
+            pltpu.VMEM((PEERS, chain, rows, wide), f32),
+            pltpu.VMEM((PEERS, chain, rows, wide), bf16),
+            pltpu.VMEM((PEERS, chain, rows, wide), bf16),
+            pltpu.VMEM((PEERS, chain, rows, wide), bf16),
+            pltpu.VMEM((PEERS, chain, rows, wide), bf16),
+            pltpu.VMEM((length // 2, hidden.shape[1]), bf16),
+            pltpu.VMEM((length // 2, hidden.shape[1]), bf16),
+            dma((2, PEERS)), dma((2, PEERS)), dma((2, PEERS)), dma((2, PEERS)),
+            dma((PEERS, chain)), dma((PEERS, chain)), dma((PEERS, chain)), dma((PEERS, chain)), dma((2,)),
+        ],
+        compiler_params=pltpu.CompilerParams(collective_id=1, has_side_effects=True),
+        cost_estimate=pl.CostEstimate(flops=1 << 32, bytes_accessed=1 << 24, transcendentals=0),
+        name="back",
+    )(queries, keys, values, out_grad, uw, inverse, dw0, start, end, beta, sums, sums_row, hidden_all, value_weight)
     grad_sums = gcol - grow.reshape(heads, length).T
     grad_log = jnp.dot(inclusive.T, grad_sums, precision=lax.Precision.HIGHEST)
     d_decay = grad_log * (-decay_rate[None, :] * jax.nn.sigmoid(decay_pre))

time: 138 us -> 120 us (0.87)
  Pallas kernels: 61.7 us -> 96.9 us
  waiting for transfers between devices: 30.5 us -> 0 us
  matrix products: 22.3 us -> 7.05 us
  starting transfers between devices: 10.9 us -> 0 us
  local copies, waits for them, and re-layouts: 8.7 us -> 12.7 us
    pallas_call x2 -> x1, Pallas kernels: 14.5 us -> 49.6 us  [compute(): pl.pallas_call(functools.partial(back_kernel, count), in_specs=[vmem] * 1...]
    ppermute x13 -> x0, waiting for transfers between devices: 30.5 us -> none  [exchange(): return lax.ppermute(value, axis, [(i, i ^ bit) for i in range(count)])]
    dot_general x8 -> x0, matrix products: 16.3 us -> none  [the longest x2 9.2 us: product(): lax.dot_general(rows, weight, (((1,), (1,)), ((), ())), preferred_element...]
    ppermute x13 -> x0, starting transfers between devices: 10.9 us -> none  [exchange(): return lax.ppermute(value, axis, [(i, i ^ bit) for i in range(count)])]
    unnamed x13 -> x12, local copies, waits for them, and re-layouts: 2.24 us -> 7.91 us
  transfers between devices with their start and end apart: 13 -> 0, of which waited for: 9 -> 0; matrix products, arithmetic and copies ran while one was open for 12% -> 0% of each run, Pallas kernels for 7% -> 0%
where the time goes in v1:
time: 120 us
  Pallas kernels  96.9 us (81%)
  local copies, waits for them, and re-layouts  12.7 us (11%)
  matrix products  7.05 us (6%)
  other arithmetic  2.46 us (2%)
    pallas_call x1, Pallas kernels, compute(): pl.pallas_call(functools.partial(back_kernel, count), in_specs=[vmem] * 1...  49.6 us
    pallas_call x1, Pallas kernels, compute(): pl.pallas_call(functools.partial(front_kernel, count), in_specs=[vmem] *...  47.2 us
    unnamed x12, local copies, waits for them, and re-layouts  7.91 us
    dot_general x1, matrix products, compute(): jnp.dot(hidden, value_weight, preferred_element_type=f32).astype(bf16)  4.56 us

profile of v1, /device:TPU:0, one launch (start us, length us, event | category | flops | bytes accessed | tf_op | source)
XLA Modules:
  0.0 119.8 jit_solution(3820155657177663387)
XLA Ops:
  0.6 0.0 copy-start
  0.6 0.7 neg.16
  1.4 1.0 fusion.1
  2.4 0.7 reshape.26.row
  3.0 0.8 copy.31.g
  3.8 0.8 copy.27
  4.6 0.7 add_divide_fusion.b
  5.3 4.6 %convolution_convert_fusion.v = bf16[256,1024]{1,0:T(8,128)(2,1)} fusion(bf16[256,2048]{1,0:T(8,128)(2,1)} %param.10, bf16[2048,1024]{1,0:T(8,128)(2,1)} %w.1), kind=kOutput, calls=%fused_computation | convolution fusion | flops 1074003968 | bytes 5767168 | tf_op jit(solution)/shard_map/dot_general | solution.py:617
  9.9 0.0 copy-done
  9.9 0.7 reshape.27
  10.7 0.4 copy.42
  11.1 1.2 %reshape.28.hid = bf16[4,256,512]{2,1,0:T(8,128)(2,1)} reshape(bf16[4,256,4,128]{3,2,1,0:T(4,128)(2,1)S(1)} %bitcast.11) | data formatting | bytes 2097152 | tf_op jit(solution)/shard_map/reshape | solution.py:629
  12.3 47.2 %front.1 = (bf16[8,256,256]{2,1,0:T(8,128)(2,1)}, f32[8,256,256]{2,1,0:T(8,128)}, f32[8,256,128]{2,1,0:T(8,128)}, bf16[8,128,128]{2,1,0:T(8,128)(2,1)}, bf16[8,1...) custom-call(bf16[256,1024]{1,0:T(8,128)(2,1)} %q.3, bf16[256,1024]{1,0:T(8,128)(2,1)} %k.3, ...), custom_call_target="tpu_custom_call" | custom-call | flops 1073741824 | bytes 8388608 | tf_op jit(solution)/shard_map/front/pallas_call | solution.py:632
  59.5 0.0 copy-start.2
  59.5 49.6 %back.1 = (bf16[256,1024]{1,0:T(8,128)(2,1)}, bf16[256,1024]{1,0:T(8,128)(2,1)}, f32[256,8]{1,0:T(8,128)}, f32[256,8]{1,0:T(8,128)}, f32[8,1,256]{2,1,0:T(1,128)...) custom-call(bf16[256,1024]{1,0:T(8,128)(2,1)} %q.3, bf16[256,1024]{1,0:T(8,128)(2,1)} %k.3, ...), custom_call_target="tpu_custom_call" | custom-call | flops 4294967296 | bytes 16777216 | tf_op jit(solution)/shard_map/back/pallas_call | solution.py:657
  109.2 0.0 copy-start.1
  109.2 1.0 subtract_multiply_fusion
  110.2 0.7 copy.35
  110.9 1.0 copy.34
  111.8 0.0 copy-done.2
  111.8 1.5 %convolution_multiply_fusion = f32[256,8]{0,1:T(8,128)} fusion(f32[256,8]{0,1:T(8,128)S(1)} %copy.34, f32[8,1,256]{2,1,0:T(1,128)} %get-tuple-element.29, f32[256,8]{0,1:T(8,128)S(1)} %copy-done.2, f32[8]{0:T(128)S(1)} %neg.16), kind=kOutput, calls=%fused_computation.1 | convolution fusion | flops 6434816 | bytes 32800 | tf_op jit(solution)/shard_map/dot_general | solution.py:685
  113.4 1.9 %copy.47 = bf16[256,1024]{1,0:T(8,128)(2,1)} copy(bf16[256,1024]{1,0:T(8,128)(2,1)} %get-tuple-element.50) | data formatting | bytes 1048576
  115.2 1.9 %copy.48 = bf16[256,1024]{1,0:T(8,128)(2,1)} copy(bf16[256,1024]{1,0:T(8,128)(2,1)} %get-tuple-element.51) | data formatting | bytes 1048576
  117.1 1.9 %copy.49 = bf16[128,2048]{1,0:T(8,128)(2,1)} copy(bf16[128,2048]{1,0:T(8,128)(2,1)} %get-tuple-element.54) | data formatting | bytes 1048576
  119.0 0.0 copy-done.1
  119.0 0.8 copy.50
Async XLA Ops:
  0.6 9.3 %copy-start = (bf16[256,2048]{1,0:T(8,128)(2,1)S(1)}, bf16[256,2048]{1,0:T(8,128)(2,1)}, u32[]{:S(2)}) copy-start(bf16[256,2048]{1,0:T(8,128)(2,1)} %param.10) | copy-start | bytes 3145732
  59.5 52.3 %copy-start.2 = (f32[256,8]{0,1:T(8,128)S(1)}, f32[256,8]{0,1:T(8,128)}, u32[]{:S(2)}) copy-start(f32[256,8]{0,1:T(8,128)} %param.13) | copy-start | bytes 24580
  109.2 9.8 %copy-start.1 = (f32[128,1024]{1,0:T(8,128)S(1)}, f32[128,1024]{1,0:T(8,128)}, u32[]{:S(2)}) copy-start(f32[128,1024]{1,0:T(8,128)} %get-tuple-element.55) | copy-start | bytes 1572868
